TPU v7x, 512 devices: a whole 4x4x16 slice. The times are simulated.
512 devices in a mesh: sp: 32 (over z, core), tp: 16 (over y, x).
Axes of the slice: x: 4, y: 4, z: 16, core: 2. Of those that a mesh axis runs over, the one named last changes fastest.
Arguments:
- tokens: bfloat16 [2, 24576, 4096], P(None, 'sp', 'tp'), may hold values from -6 to 6
- w_key: bfloat16 [4096, 2048], P(None, 'tp'), may hold values from -0.09375 to 0.09375
- w_value: bfloat16 [4096, 2048], P(None, 'tp'), may hold values from -0.09375 to 0.09375
- w_gate: bfloat16 [4096, 4, 16], replicated, may hold values from -0.09375 to 0.09375
- forget_bias: float32 [2, 16], replicated, may hold values from 3.9 to 13, as said below
- log_shift: float32 [2, 4, 16, 24576], P(None, None, 'tp', 'sp'), may hold values from -5 to 121, as said below
- new_query: bfloat16 [2, 4096, 2048], P(None, 'sp', 'tp'), may hold values from -6 to 6
Outputs:
- cache_matrix: bfloat16 [2, 2, 16, 128, 128], P(None, None, 'tp')
- cache_norm: float32 [2, 2, 16, 128], P(None, None, 'tp')
- cache_max: float32 [2, 2, 16], P(None, None, 'tp')
- first_read: bfloat16 [2, 4096, 2048], P(None, 'sp', 'tp')
Inputs may be any that keep to these rules, and one draw needn't show every extreme that they name: `forget_bias`: added to the forget gates' pre-activations, by direction and head. `log_shift`: rows 0 and 2 are added to the input gates of the two directions; rows 1 and 3 are added to the log forget gates and are never positive.
All inputs are finite; a program needn't handle non-finite values.
Results may differ from a plain program's by a relative error of at most 0.024.
Values may be sent and summed in bfloat16 or wider, within the bound.
No kernel may reach another device: no remote copies, remote signals or barrier semaphores. Data moves between devices by JAX's collectives and lax.ppermute only.
A program may use at most 64 MiB of HBM per device.

v0:
```python
import functools

import jax
import jax.numpy as jnp
from jax import lax
from jax.experimental import pallas as pl
from jax.experimental.pallas import tpu as pltpu
from jax.sharding import Mesh
from jax.sharding import PartitionSpec as P


HEAD = 128
SP = ("za", "zb", "c")
GROUP = ("zb", "c")
F32 = jnp.float32
BF16 = jnp.bfloat16


def shifted(array, core_axis, k):
    pairs = []
    for c in range(2):
        for y in range(4):
            for x in range(4):
                along_x = c == core_axis
                to = (y, (x + k) % 4) if along_x else ((y + k) % 4, x)
                pairs.append((c * 16 + y * 4 + x, c * 16 + to[0] * 4 + to[1]))
    return lax.ppermute(array, ("c", "y", "x"), pairs)


def gather_from(array, k):
    return shifted(array, 0, k)


def scatter_to(array, k):
    return shifted(array, 1, k)


def where_am_i():
    return lax.axis_index("c"), lax.axis_index("y"), lax.axis_index("x")


def feature_block(c, y, x, k, j):
    return jnp.where(c == 0, ((y + k) % 4) * 4 + (x - j + 4) % 4, ((y - j + 4) % 4) * 4 + (x + k) % 4)


def scatter_head(c, y, x, k):
    return jnp.where(c == 0, ((y + k) % 4) * 4 + x, y * 4 + (x + k) % 4)


def exchange(array, axes):
    return lax.all_to_all(array, axes, 0, 0, tiled=True)


def call(kernel, out_shape, flops=1000000, **more):
    return pl.pallas_call(
        kernel,
        out_shape=out_shape,
        cost_estimate=pl.CostEstimate(flops=flops, bytes_accessed=1000000, transcendentals=0),
        compiler_params=pltpu.CompilerParams(vmem_limit_bytes=48 * 1024 * 1024),
        **more,
    )


def shape(*dims, dtype=BF16):
    return jax.ShapeDtypeStruct(dims, dtype)


def pack_weights_kernel(wk_ref, wv_ref, *out_refs):
    c, y, x = where_am_i()
    part = out_refs[0].shape[0] // 4
    for k, out in enumerate(out_refs):
        for j in range(4):
            rows = pl.ds(feature_block(c, y, x, k, j) * part, part)
            out[j * part : (j + 1) * part, 0:128] = wk_ref[rows, :]
            out[j * part : (j + 1) * part, 128:256] = wv_ref[rows, :]


def pair_rows(values):
    row = lax.broadcasted_iota(jnp.int32, values.shape, 0)
    high = values.astype(BF16).astype(F32)
    return jnp.where(row < 4, high, values - high)


def store_gates(ref, p, top, values):
    paired = pair_rows(values)
    blocks = [paired[:, 256 * b : 256 * b + 256] for b in range(paired.shape[1] // 256)]
    blocks.append(jnp.zeros_like(blocks[0]))
    ref[p, top : top + 32, :] = jnp.concatenate(blocks, axis=0).astype(BF16)


def load_gates(tile):
    wide = tile.astype(F32)
    paired = jnp.concatenate([wide[8 * b : 8 * b + 8] for b in range(3)], axis=1)
    return paired + pltpu.roll(paired, 4, 0)


def gates_kernel(t0_ref, t1_ref, t2_ref, t3_ref, gate_ref, out_ref):
    c, y, x = where_am_i()
    weight = jnp.concatenate([gate_ref[feature_block(c, y, x, 0, j)] for j in range(4)], axis=1)
    for p in range(t0_ref.shape[0]):
        piece = jnp.concatenate([t[p] for t in (t0_ref, t1_ref, t2_ref, t3_ref)], axis=1)
        out_ref[p] = lax.dot_general(weight, piece, (((1,), (1,)), ((), ())), preferred_element_type=F32)


def project_kernel(k, t0_ref, t1_ref, t2_ref, t3_ref, w_ref, gates_ref, out_ref):
    c, y, x = where_am_i()
    rows = t0_ref.shape[1]
    for p in range(t0_ref.shape[0]):
        piece = jnp.concatenate([t[p] for t in (t0_ref, t1_ref, t2_ref, t3_ref)], axis=1)
        total = jnp.dot(piece, w_ref[...], preferred_element_type=F32)
        out_ref[p, 0:rows, :] = total.astype(BF16)
        store_gates(out_ref, p, rows, gates_ref[p, pl.ds(scatter_head(c, y, x, k) * 8, 8), :])


def log_sigmoid(v):
    return jnp.minimum(v, 0.0) - jnp.log1p(jnp.exp(-jnp.abs(v)))


def local_state(head, prompt, bias_ref, shift_ref, pieces):
    rows = shift_ref.shape[3]
    total = sum(ref[prompt, 0:rows, :].astype(F32) for ref in pieces)
    gates = sum(load_gates(ref[prompt, rows : rows + 32, :]) for ref in pieces)
    keys = total[:, 0:128].astype(BF16)
    values = total[:, 128:256].astype(BF16)
    length = gates.shape[1]
    shift = shift_ref[prompt, :, 0, :]
    row4 = lax.broadcasted_iota(jnp.int32, (4, length), 0)
    bias = jnp.where(row4 == 1, bias_ref[0, head], bias_ref[1, head])
    gates = gates[0:4, :]
    entry = gates + shift
    forget = log_sigmoid(gates + bias) + shift
    blocks = length // 128
    tall = jnp.concatenate([forget[:, 128 * b : 128 * b + 128] for b in range(blocks)], axis=0)
    r = lax.broadcasted_iota(jnp.int32, (128, 128), 0)
    c = lax.broadcasted_iota(jnp.int32, (128, 128), 1)
    climb = jnp.dot(tall, (r <= c).astype(F32), precision=lax.Precision.HIGHEST, preferred_element_type=F32)
    carry = jnp.zeros((4, 1), F32)
    parts = []
    for b in range(blocks):
        block = climb[4 * b : 4 * b + 4, :]
        parts.append(block + carry)
        carry = carry + block[:, 127:128]
    climb = jnp.concatenate(parts, axis=1)
    weight_fwd = carry[1:2] - climb[1:2] + entry[0:1]
    weight_bwd = climb[3:4] - forget[3:4] + entry[2:3]
    keys_t = jnp.transpose(keys.astype(F32))
    scale = HEAD ** -0.5
    memories, norms, tops, totals = [], [], [], []
    for weight, total in ((weight_fwd, carry[1:2]), (weight_bwd, carry[3:4])):
        top = jnp.max(weight, axis=1, keepdims=True)
        now = jnp.exp(weight - top)
        weighted = (keys_t * now).astype(BF16)
        memories.append(jnp.dot(weighted, values, preferred_element_type=F32) * scale)
        high = now.astype(BF16)
        low = (now - high.astype(F32)).astype(BF16)
        both = jnp.concatenate([high, low, jnp.zeros((6, length), BF16)], axis=0)
        norm = jnp.dot(both, keys, preferred_element_type=F32)
        norms.append((norm[0:1] + norm[1:2]) * scale)
        tops.append(jnp.broadcast_to(top, (1, 128)))
        totals.append(jnp.broadcast_to(total, (1, 128)))
    return memories, norms, totals, tops


def split_three(values):
    high = values.astype(BF16).astype(F32)
    rest = values - high
    middle = rest.astype(BF16).astype(F32)
    return high, middle, rest - middle


def small_tile(norms, totals, tops):
    norm_high = norms.astype(BF16).astype(F32)
    parts = split_three(jnp.concatenate([totals, tops], axis=0))
    return jnp.concatenate([norm_high, norms - norm_high, *parts], axis=0).astype(BF16)


def state_kernel(bias_ref, shift_ref, a_ref, b_ref, c_ref, d_ref, out_ref):
    head = lax.axis_index("y") * 4 + lax.axis_index("x")
    memories, norms, totals, tops = [], [], [], []
    for p in range(2):
        found = local_state(head, p, bias_ref, shift_ref, (a_ref, b_ref, c_ref, d_ref))
        for have, more in zip((memories, norms, totals, tops), found):
            have.extend(more)
    tile = small_tile(*(jnp.concatenate(v, axis=0) for v in (norms, totals, tops)))
    for g in range(8):
        for i in range(4):
            out_ref[g, 16 * i : 16 * i + 16, :] = memories[i][16 * g : 16 * g + 16, :].astype(BF16)
        out_ref[g, 64:96, :] = tile


def merged(in_ref, count):
    tiles = [in_ref[g, 64:96, :].astype(F32) for g in range(count)]
    norms = [t[0:4] + t[4:8] for t in tiles]
    scalars = [t[8:16] + t[16:24] + t[24:32] for t in tiles]
    totals = [s[0:4] for s in scalars]
    tops = [s[4:8] for s in scalars]
    row = lax.broadcasted_iota(jnp.int32, (4, 128), 0)
    before, after = [jnp.zeros((4, 128), F32)], [jnp.zeros((4, 128), F32)]
    for g in range(count - 1):
        before.append(before[-1] + totals[g])
        after.append(after[-1] + totals[count - 1 - g])
    whole = before[-1] + totals[-1]
    after = after[::-1]
    tops = [t + jnp.where(row % 2 == 0, after[g], before[g]) for g, t in enumerate(tops)]
    top = tops[0]
    for t in tops[1:]:
        top = jnp.maximum(top, t)
    return norms, tops, whole, top


def weighted_sums(in_ref, count, norms, tops, top):
    factors = [jnp.exp(t - top) for t in tops]
    norm = sum(f * n for f, n in zip(factors, norms))
    blocks = []
    for i in range(4):
        total = jnp.zeros((16, 128), F32)
        for g in range(count):
            total = total + in_ref[g, 16 * i : 16 * i + 16, :].astype(F32) * factors[g][i : i + 1]
        blocks.append(total)
    return norm, blocks


def group_merge_kernel(in_ref, out_ref):
    norms, tops, whole, top = merged(in_ref, 8)
    norm, blocks = weighted_sums(in_ref, 8, norms, tops, top)
    tile = small_tile(norm, whole, top)
    for g in range(4):
        for i in range(4):
            out_ref[g, 16 * i : 16 * i + 16, :] = blocks[i].astype(BF16)
        out_ref[g, 64:96, :] = tile


def last_merge_kernel(in_ref, out_ref, norm_ref, max_ref):
    norms, tops, whole, top = merged(in_ref, 4)
    top = jnp.maximum(whole, top)
    norm, blocks = weighted_sums(in_ref, 4, norms, tops, top)
    for g in range(8):
        for i in range(4):
            out_ref[g, 16 * i : 16 * i + 16, :] = blocks[i].astype(BF16)
    norm_ref[...] = norm
    max_ref[...] = top


def read_kernel(in_ref, norm_ref, query_ref, matrix_ref, read_ref):
    for g in range(8):
        for i in range(4):
            matrix_ref[i // 2, i % 2, 0, 16 * g : 16 * g + 16, :] = in_ref[g, 16 * i : 16 * i + 16, :]
    for p in range(2):
        query = query_ref[p]
        wide = query.astype(F32)
        total = jnp.zeros(wide.shape, F32)
        for j in range(2):
            i = 2 * p + j
            numerator = jnp.dot(query, matrix_ref[p, j, 0], preferred_element_type=F32)
            inner = jnp.sum(wide * norm_ref[i : i + 1, :], axis=1, keepdims=True)
            total = total + numerator / jnp.maximum(jnp.abs(inner), 1.0)
        read_ref[p] = total.astype(BF16)


def program(tokens, w_key, w_value, w_gate, forget_bias, log_shift, new_query):
    prompts, length, width = tokens.shape
    depth = 4 * width
    pieces = [tokens] + [gather_from(tokens, k) for k in (1, 2, 3)]
    weights = call(pack_weights_kernel, (shape(depth, 2 * HEAD),) * 4)(w_key, w_value)
    weights = [weights[0]] + [scatter_to(weights[k], k) for k in (1, 2, 3)]
    weights = [weights[0], weights[3], weights[2], weights[1]]
    gate = w_gate.transpose(2, 1, 0)
    gate = jnp.concatenate([gate, gate], axis=1).reshape(128, 16, width).transpose(1, 0, 2)
    gates = call(gates_kernel, shape(prompts, 128, length, dtype=F32))(*pieces, gate)
    partial = []
    for k in range(4):
        project = call(
            functools.partial(project_kernel, k),
            shape(prompts, length + 32, 2 * HEAD),
            flops=2 * prompts * length * depth * 256,
        )
        part = project(*pieces, weights[k], gates)
        partial.append(scatter_to(part, k) if k else part)
    smem = pl.BlockSpec(memory_space=pltpu.SMEM)
    vmem = pl.BlockSpec(memory_space=pltpu.VMEM)
    packed = call(state_kernel, shape(8, 96, HEAD), in_specs=[smem] + [vmem] * 5)(forget_bias, log_shift, *partial)
    grouped = call(group_merge_kernel, shape(4, 96, HEAD))(exchange(packed, GROUP))
    slices, norm, top = call(
        last_merge_kernel, (shape(8, 64, HEAD), shape(4, HEAD, dtype=F32), shape(4, HEAD, dtype=F32))
    )(exchange(grouped, "za"))
    matrix, read = call(read_kernel, (shape(2, 2, 1, HEAD, HEAD), shape(*new_query.shape)))(
        exchange(slices, GROUP), norm, new_query
    )
    return matrix, norm.reshape(2, 2, 1, HEAD), top[:, 0].reshape(2, 2, 1), read


def solution(mesh):
    finer = Mesh(mesh.devices.reshape(4, 4, 2, 4, 4), ("za", "zb", "c", "y", "x"))
    tp = ("y", "x")
    in_specs = (
        P(None, SP, tp),
        P(None, tp),
        P(None, tp),
        P(),
        P(),
        P(None, None, tp, SP),
        P(None, SP, tp),
    )
    out_specs = (
        P(None, None, tp, None, None),
        P(None, None, tp, None),
        P(None, None, tp),
        P(None, SP, tp),
    )
    return jax.shard_map(program, mesh=finer, in_specs=in_specs, out_specs=out_specs, check_vma=False)
```

profile of v0, /device:TPU:1, one launch (start us, length us, event | category | flops | bytes accessed | tf_op | source)
XLA Modules:
  0.0 125.9 jit_solution(15810698869756193379)
XLA Ops:
  0.6 5.5 %collective-permute-start.2 = (bf16[2,768,256]{2,1,0:T(8,128)(2,1)}, bf16[2,768,256]{2,1,0:T(8,128)(2,1)S(1)}, u32[]{:S(2)}, u32[]{:S(2)}) collective-permute-start(bf16[2,768,256]{2,1,0:T(8,128)(2,1)} %t0_ref.9), channel_id=1, source_target_pairs={{0,3},{1,0},{2,1},{3,2},{4,7},{5,4},{6,5},{7,6},{8,11},{9,8},{10,9... | collective-permute-start | bytes 2359304 | tf_op jit(solution)/shard_map/ppermute | solution.py:27
  6.1 2.3 %collective-permute-start.1 = (bf16[2,768,256]{2,1,0:T(8,128)(2,1)}, bf16[2,768,256]{2,1,0:T(8,128)(2,1)S(1)}, u32[]{:S(2)}, u32[]{:S(2)}) collective-permute-start(bf16[2,768,256]{2,1,0:T(8,128)(2,1)} %t0_ref.9), channel_id=1, source_target_pairs={{0,2},{1,3},{2,0},{3,1},{4,6},{5,7},{6,4},{7,5},{8,10},{9,11},{10,... | collective-permute-start | bytes 2359304 | tf_op jit(solution)/shard_map/ppermute | solution.py:27
  8.4 2.6 %collective-permute-start = (bf16[2,768,256]{2,1,0:T(8,128)(2,1)}, bf16[2,768,256]{2,1,0:T(8,128)(2,1)S(1)}, u32[]{:S(2)}, u32[]{:S(2)}) collective-permute-start(bf16[2,768,256]{2,1,0:T(8,128)(2,1)} %t0_ref.9), channel_id=1, source_target_pairs={{0,1},{1,2},{2,3},{3,0},{4,5},{5,6},{6,7},{7,4},{8,9},{9,10},{10,1... | collective-permute-start | bytes 2359304 | tf_op jit(solution)/shard_map/ppermute | solution.py:27
  11.0 1.2 copy-done.1
  12.2 1.2 copy-done.2
  13.8 3.1 %collective-permute-start.7 = (bf16[1024,256]{1,0:T(8,128)(2,1)S(1)}, bf16[1024,256]{1,0:T(8,128)(2,1)S(1)}, u32[]{:S(2)}, u32[]{:S(2)}) collective-permute-start(bf16[1024,256]{1,0:T(8,128)(2,1)S(1)} %get-tuple-element.16), channel_id=1, source_target_pairs={{0,4},{1,5},{2,6},{3,7},{4,8},{5,9},{6,10},{7,11},{8,12},{9,13},{1... | collective-permute-start | bytes 1572872 | tf_op jit(solution)/shard_map/ppermute | solution.py:27
  16.9 3.4 %collective-permute-start.3 = (bf16[1024,256]{1,0:T(8,128)(2,1)S(1)}, bf16[1024,256]{1,0:T(8,128)(2,1)S(1)}, u32[]{:S(2)}, u32[]{:S(2)}) collective-permute-start(bf16[1024,256]{1,0:T(8,128)(2,1)S(1)} %get-tuple-element.14), channel_id=1, source_target_pairs={{0,12},{1,13},{2,14},{3,15},{4,0},{5,1},{6,2},{7,3},{8,4},{9,5},{1... | collective-permute-start | bytes 1572872 | tf_op jit(solution)/shard_map/ppermute | solution.py:27
  20.3 3.4 %collective-permute-done.2.t3_ref = bf16[2,768,256]{2,1,0:T(8,128)(2,1)S(1)} collective-permute-done((bf16[2,768,256]{2,1,0:T(8,128)(2,1)}, bf16[2,768,256]{2,1,0:T(8,128)(2,1)S(1)}, u32[]{:S(2)}, u32[]{:S(2)}) %collective-permute-start.2) | collective-permute-done | bytes 786464 | tf_op jit(solution)/shard_map/ppermute | solution.py:27
  23.8 4.6 %collective-permute-start.5 = (bf16[1024,256]{1,0:T(8,128)(2,1)S(1)}, bf16[1024,256]{1,0:T(8,128)(2,1)S(1)}, u32[]{:S(2)}, u32[]{:S(2)}) collective-permute-start(bf16[1024,256]{1,0:T(8,128)(2,1)S(1)} %get-tuple-element.15), channel_id=1, source_target_pairs={{0,8},{1,9},{2,10},{3,11},{4,12},{5,13},{6,14},{7,15},{8,0},{9,1},... | collective-permute-start | bytes 1572872 | tf_op jit(solution)/shard_map/ppermute | solution.py:27
  29.7 4.7 %collective-permute-done.t1_ref = bf16[2,768,256]{2,1,0:T(8,128)(2,1)S(1)} collective-permute-done((bf16[2,768,256]{2,1,0:T(8,128)(2,1)}, bf16[2,768,256]{2,1,0:T(8,128)(2,1)S(1)}, u32[]{:S(2)}, u32[]{:S(2)}) %collective-permute-start) | collective-permute-done | bytes 786464 | tf_op jit(solution)/shard_map/ppermute | solution.py:27
  34.4 1.1 shard_map.103.gates_ref
  35.6 4.3 %collective-permute-done.7.w_ref = bf16[1024,256]{1,0:T(8,128)(2,1)S(1)} collective-permute-done((bf16[1024,256]{1,0:T(8,128)(2,1)S(1)}, bf16[1024,256]{1,0:T(8,128)(2,1)S(1)}, u32[]{:S(2)}, u32[]{:S(2)}) %collective-permute-start.7) | collective-permute-done | bytes 524320 | tf_op jit(solution)/shard_map/ppermute | solution.py:27
  40.9 1.9 %collective-permute-start.8 = (bf16[2,800,256]{2,1,0:T(8,128)(2,1)S(1)}, bf16[2,800,256]{2,1,0:T(8,128)(2,1)S(1)}, u32[]{:S(2)}, u32[]{:S(2)}) collective-permute-start(bf16[2,800,256]{2,1,0:T(8,128)(2,1)S(1)} %shard_map.107), channel_id=1, source_target_pairs={{0,12},{1,13},{2,14},{3,15},{4,0},{5,1},{6,2},{7,3},{8,4},{9,5},{1... | collective-permute-start | bytes 2457608 | tf_op jit(solution)/shard_map/ppermute | solution.py:27
  42.8 1.0 shard_map.106
  43.8 2.7 %collective-permute-start.6 = (bf16[2,800,256]{2,1,0:T(8,128)(2,1)S(1)}, bf16[2,800,256]{2,1,0:T(8,128)(2,1)S(1)}, u32[]{:S(2)}, u32[]{:S(2)}) collective-permute-start(bf16[2,800,256]{2,1,0:T(8,128)(2,1)S(1)} %shard_map.106), channel_id=1, source_target_pairs={{0,8},{1,9},{2,10},{3,11},{4,12},{5,13},{6,14},{7,15},{8,0},{9,1},... | collective-permute-start | bytes 2457608 | tf_op jit(solution)/shard_map/ppermute | solution.py:27
  47.4 2.6 %collective-permute-start.4 = (bf16[2,800,256]{2,1,0:T(8,128)(2,1)S(1)}, bf16[2,800,256]{2,1,0:T(8,128)(2,1)S(1)}, u32[]{:S(2)}, u32[]{:S(2)}) collective-permute-start(bf16[2,800,256]{2,1,0:T(8,128)(2,1)S(1)} %shard_map.105), channel_id=1, source_target_pairs={{0,4},{1,5},{2,6},{3,7},{4,8},{5,9},{6,10},{7,11},{8,12},{9,13},{1... | collective-permute-start | bytes 2457608 | tf_op jit(solution)/shard_map/ppermute | solution.py:27
  51.1 3.2 %collective-permute-done.8.d_ref = bf16[2,800,256]{2,1,0:T(8,128)(2,1)S(1)} collective-permute-done((bf16[2,800,256]{2,1,0:T(8,128)(2,1)S(1)}, bf16[2,800,256]{2,1,0:T(8,128)(2,1)S(1)}, u32[]{:S(2)}, u32[]{:S(2)}) %collective-permute-start.8) | collective-permute-done | bytes 819232 | tf_op jit(solution)/shard_map/ppermute | solution.py:27
  54.2 4.5 %collective-permute-done.6.c_ref = bf16[2,800,256]{2,1,0:T(8,128)(2,1)S(1)} collective-permute-done((bf16[2,800,256]{2,1,0:T(8,128)(2,1)S(1)}, bf16[2,800,256]{2,1,0:T(8,128)(2,1)S(1)}, u32[]{:S(2)}, u32[]{:S(2)}) %collective-permute-start.6) | collective-permute-done | bytes 819232 | tf_op jit(solution)/shard_map/ppermute | solution.py:27
  58.7 8.7 %collective-permute-done.4.b_ref = bf16[2,800,256]{2,1,0:T(8,128)(2,1)S(1)} collective-permute-done((bf16[2,800,256]{2,1,0:T(8,128)(2,1)S(1)}, bf16[2,800,256]{2,1,0:T(8,128)(2,1)S(1)}, u32[]{:S(2)}, u32[]{:S(2)}) %collective-permute-start.4) | collective-permute-done | bytes 819232 | tf_op jit(solution)/shard_map/ppermute | solution.py:27
  67.4 1.9 %shard_map.108 = bf16[8,96,128]{2,1,0:T(8,128)(2,1)S(1)} custom-call(f32[2,16]{1,0:T(2,128)S(1)} %copy-done.6, f32[2,4,1,768]{3,2,1,0:T(1,128)S(1)} %copy-done.4, bf16[2,800,256]{2,1,0:T(8,128)(2,1)S(1)} %shard_map.104.a_ref, bf16[2,800,256]{2,1,0:T(8,128)(2,1)S(1)} %collective-permute-done.4.b_ref, bf16[2,800,256]{2,1,0:T(8,128)(2,1)S(1)} %collective-permute-done.6.c_ref, ...), custom_call_target="tpu_custom_call" | custom-call | flops 1000000 | bytes 1000000 | tf_op jit(solution)/shard_map/pallas_call | solution.py:281
  69.4 18.2 %all_to_all.15.in_ref = bf16[8,96,128]{2,1,0:T(8,128)(2,1)S(1)} all-to-all(bf16[8,96,128]{2,1,0:T(8,128)(2,1)S(1)} %shard_map.108), channel_id=1, replica_groups=mesh['za'=4,'zb'=4,'c'=2,'y'=4,'x'=4] {'zb','c'}, dimensions={0} | all-to-all | bytes 393216 | tf_op jit(solution)/shard_map/all_to_all | solution.py:51
  87.7 23.9 %all_to_all.16.in_ref = bf16[4,96,128]{2,1,0:T(8,128)(2,1)S(1)} all-to-all(bf16[4,96,128]{2,1,0:T(8,128)(2,1)S(1)} %shard_map.109), channel_id=1, replica_groups=mesh['za'=4,'zb'=4,'c'=2,'y'=4,'x'=4] {'za'}, dimensions={0} | all-to-all | bytes 196608 | tf_op jit(solution)/shard_map/all_to_all | solution.py:51
  112.3 7.0 %all-to-all-start.2 = ((bf16[8,64,128]{2,1,0:T(8,128)(2,1)}), bf16[8,64,128]{2,1,0:T(8,128)(2,1)S(1)}, u32[]{:S(2)}, u32[]{:S(2)}) async-start(bf16[8,64,128]{2,1,0:T(8,128)(2,1)} %get-tuple-element.17), calls=%async_computation.2 | async-start | bytes 262144 | tf_op jit(solution)/shard_map/all_to_all | solution.py:51
  120.0 5.0 %all-to-all-done.2.in_ref = bf16[8,64,128]{2,1,0:T(8,128)(2,1)S(1)} async-done(((bf16[8,64,128]{2,1,0:T(8,128)(2,1)}), bf16[8,64,128]{2,1,0:T(8,128)(2,1)S(1)}, u32[]{:S(2)}, u32[]{:S(2)}) %all-to-all-start.2) | async-done | bytes 131104 | tf_op jit(solution)/shard_map/all_to_all | solution.py:51
  (30 shorter events, 6.9 us)
Async XLA Ops:
  0.6 23.1 %collective-permute-start.2 = (bf16[2,768,256]{2,1,0:T(8,128)(2,1)}, bf16[2,768,256]{2,1,0:T(8,128)(2,1)S(1)}, u32[]{:S(2)}, u32[]{:S(2)}) collective-permute-start(bf16[2,768,256]{2,1,0:T(8,128)(2,1)} %t0_ref.9), channel_id=1, source_target_pairs={{0,3},{1,0},{2,1},{3,2},{4,7},{5,4},{6,5},{7,6},{8,11},{9,8},{10,9... | collective-permute-start | bytes 2359304 | tf_op jit(solution)/shard_map/ppermute | solution.py:27
  6.1 23.6 %collective-permute-start.1 = (bf16[2,768,256]{2,1,0:T(8,128)(2,1)}, bf16[2,768,256]{2,1,0:T(8,128)(2,1)S(1)}, u32[]{:S(2)}, u32[]{:S(2)}) collective-permute-start(bf16[2,768,256]{2,1,0:T(8,128)(2,1)} %t0_ref.9), channel_id=1, source_target_pairs={{0,2},{1,3},{2,0},{3,1},{4,6},{5,7},{6,4},{7,5},{8,10},{9,11},{10,... | collective-permute-start | bytes 2359304 | tf_op jit(solution)/shard_map/ppermute | solution.py:27
  8.4 26.1 %collective-permute-start = (bf16[2,768,256]{2,1,0:T(8,128)(2,1)}, bf16[2,768,256]{2,1,0:T(8,128)(2,1)S(1)}, u32[]{:S(2)}, u32[]{:S(2)}) collective-permute-start(bf16[2,768,256]{2,1,0:T(8,128)(2,1)} %t0_ref.9), channel_id=1, source_target_pairs={{0,1},{1,2},{2,3},{3,0},{4,5},{5,6},{6,7},{7,4},{8,9},{9,10},{10,1... | collective-permute-start | bytes 2359304 | tf_op jit(solution)/shard_map/ppermute | solution.py:27
  11.0 1.2 copy-start.1
  12.2 1.2 copy-start.2
  13.4 15.0 %copy-start.7 = (bf16[4096,4,16]{0,2,1:T(8,128)(2,1)S(1)}, bf16[4096,4,16]{0,2,1:T(8,128)(2,1)}, u32[]{:S(2)}) copy-start(bf16[4096,4,16]{0,2,1:T(8,128)(2,1)} %param.10) | copy-start | bytes 1572868
  13.8 26.1 %collective-permute-start.7 = (bf16[1024,256]{1,0:T(8,128)(2,1)S(1)}, bf16[1024,256]{1,0:T(8,128)(2,1)S(1)}, u32[]{:S(2)}, u32[]{:S(2)}) collective-permute-start(bf16[1024,256]{1,0:T(8,128)(2,1)S(1)} %get-tuple-element.16), channel_id=1, source_target_pairs={{0,4},{1,5},{2,6},{3,7},{4,8},{5,9},{6,10},{7,11},{8,12},{9,13},{1... | collective-permute-start | bytes 1572872 | tf_op jit(solution)/shard_map/ppermute | solution.py:27
  16.9 29.5 %collective-permute-start.3 = (bf16[1024,256]{1,0:T(8,128)(2,1)S(1)}, bf16[1024,256]{1,0:T(8,128)(2,1)S(1)}, u32[]{:S(2)}, u32[]{:S(2)}) collective-permute-start(bf16[1024,256]{1,0:T(8,128)(2,1)S(1)} %get-tuple-element.14), channel_id=1, source_target_pairs={{0,12},{1,13},{2,14},{3,15},{4,0},{5,1},{6,2},{7,3},{8,4},{9,5},{1... | collective-permute-start | bytes 1572872 | tf_op jit(solution)/shard_map/ppermute | solution.py:27
  23.8 19.0 %collective-permute-start.5 = (bf16[1024,256]{1,0:T(8,128)(2,1)S(1)}, bf16[1024,256]{1,0:T(8,128)(2,1)S(1)}, u32[]{:S(2)}, u32[]{:S(2)}) collective-permute-start(bf16[1024,256]{1,0:T(8,128)(2,1)S(1)} %get-tuple-element.15), channel_id=1, source_target_pairs={{0,8},{1,9},{2,10},{3,11},{4,12},{5,13},{6,14},{7,15},{8,0},{9,1},... | collective-permute-start | bytes 1572872 | tf_op jit(solution)/shard_map/ppermute | solution.py:27
  29.4 5.1 %copy-start = (bf16[2,768,256]{2,1,0:T(8,128)(2,1)S(1)}, bf16[2,768,256]{2,1,0:T(8,128)(2,1)}, u32[]{:S(2)}) copy-start(bf16[2,768,256]{2,1,0:T(8,128)(2,1)} %t0_ref.9) | copy-start | bytes 2359300
  40.9 13.4 %collective-permute-start.8 = (bf16[2,800,256]{2,1,0:T(8,128)(2,1)S(1)}, bf16[2,800,256]{2,1,0:T(8,128)(2,1)S(1)}, u32[]{:S(2)}, u32[]{:S(2)}) collective-permute-start(bf16[2,800,256]{2,1,0:T(8,128)(2,1)S(1)} %shard_map.107), channel_id=1, source_target_pairs={{0,12},{1,13},{2,14},{3,15},{4,0},{5,1},{6,2},{7,3},{8,4},{9,5},{1... | collective-permute-start | bytes 2457608 | tf_op jit(solution)/shard_map/ppermute | solution.py:27
  43.8 14.9 %collective-permute-start.6 = (bf16[2,800,256]{2,1,0:T(8,128)(2,1)S(1)}, bf16[2,800,256]{2,1,0:T(8,128)(2,1)S(1)}, u32[]{:S(2)}, u32[]{:S(2)}) collective-permute-start(bf16[2,800,256]{2,1,0:T(8,128)(2,1)S(1)} %shard_map.106), channel_id=1, source_target_pairs={{0,8},{1,9},{2,10},{3,11},{4,12},{5,13},{6,14},{7,15},{8,0},{9,1},... | collective-permute-start | bytes 2457608 | tf_op jit(solution)/shard_map/ppermute | solution.py:27
  47.4 20.0 %collective-permute-start.4 = (bf16[2,800,256]{2,1,0:T(8,128)(2,1)S(1)}, bf16[2,800,256]{2,1,0:T(8,128)(2,1)S(1)}, u32[]{:S(2)}, u32[]{:S(2)}) collective-permute-start(bf16[2,800,256]{2,1,0:T(8,128)(2,1)S(1)} %shard_map.105), channel_id=1, source_target_pairs={{0,4},{1,5},{2,6},{3,7},{4,8},{5,9},{6,10},{7,11},{8,12},{9,13},{1... | collective-permute-start | bytes 2457608 | tf_op jit(solution)/shard_map/ppermute | solution.py:27
  50.1 17.4 %copy-start.4 = (f32[2,4,1,768]{3,2,1,0:T(1,128)S(1)}, f32[2,4,1,768]{3,2,1,0:T(1,128)}, u32[]{:S(2)}) copy-start(f32[2,4,1,768]{3,2,1,0:T(1,128)} %shift_ref.1) | copy-start | bytes 73732
  50.1 17.4 %copy-start.6 = (f32[2,16]{1,0:T(2,128)S(1)}, f32[2,16]{1,0:T(2,128)}, u32[]{:S(2)}) copy-start(f32[2,16]{1,0:T(2,128)} %bias_ref.1) | copy-start | bytes 388
  112.3 12.8 %copy-start.3 = (bf16[2,128,128]{2,1,0:T(8,128)(2,1)S(1)}, bf16[2,128,128]{2,1,0:T(8,128)(2,1)}, u32[]{:S(2)}) copy-start(bf16[2,128,128]{2,1,0:T(8,128)(2,1)} %query_ref.1) | copy-start | bytes 196612
  112.3 12.8 %all-to-all-start.2 = ((bf16[8,64,128]{2,1,0:T(8,128)(2,1)}), bf16[8,64,128]{2,1,0:T(8,128)(2,1)S(1)}, u32[]{:S(2)}, u32[]{:S(2)}) async-start(bf16[8,64,128]{2,1,0:T(8,128)(2,1)} %get-tuple-element.17), calls=%async_computation.2 | async-start | bytes 262144 | tf_op jit(solution)/shard_map/all_to_all | solution.py:51
  119.4 5.7 %copy-start.5 = (f32[4,128]{1,0:T(4,128)S(1)}, f32[4,128]{1,0:T(4,128)}, u32[]{:S(2)}) copy-start(f32[4,128]{1,0:T(4,128)} %get-tuple-element.18.norm_ref) | copy-start | bytes 6148
where the time goes:
time: 126 us
  blocking collectives  42.1 us (33%)
  starting transfers between devices  35.7 us (28%)
  waiting for transfers between devices  33.8 us (27%)
  Pallas kernels  8.91 us (7%)
  local copies, waits for them, and re-layouts  4.4 us (3%)
    all_to_all x2, blocking collectives, exchange(): return lax.all_to_all(array, axes, 0, 0, tiled=True)  42.1 us
    ppermute x9, waiting for transfers between devices, shifted(): return lax.ppermute(array, ('c', 'y', 'x'), pairs)  28.8 us
    ppermute x9, starting transfers between devices, shifted(): return lax.ppermute(array, ('c', 'y', 'x'), pairs)  28.7 us
    all_to_all x1, starting transfers between devices, exchange(): return lax.all_to_all(array, axes, 0, 0, tiled=True)  6.99 us
    all_to_all x1, waiting for transfers between devices, exchange(): return lax.all_to_all(array, axes, 0, 0, tiled=True)  5.02 us
    pallas_call x4, Pallas kernels, program(): part = project(*pieces, weights[k], gates)  3.87 us
    unnamed x17, local copies, waits for them, and re-layouts  2.72 us
  transfers between devices with their start and end apart: 10, of which 7 were waited for; matrix products, arithmetic and copies ran while one was open for 2% of the time, Pallas kernels for 4%

commit v1 on v0

--- a/solution.py
+++ b/solution.py
@@ -94,19 +94,26 @@
     return paired + pltpu.roll(paired, 4, 0)
 
 
-def gates_kernel(t0_ref, t1_ref, t2_ref, t3_ref, gate_ref, out_ref):
+def joined(p, t0_ref, t1_ref, far_a_ref, far_b_ref, t3_ref):
+    far_ref = far_b_ref if p else far_a_ref
+    return jnp.concatenate([t0_ref[p], t1_ref[p], far_ref[0], t3_ref[p]], axis=1)
+
+
+def gates_kernel(*refs):
+    *piece_refs, gate_ref, out_ref = refs
     c, y, x = where_am_i()
     weight = jnp.concatenate([gate_ref[feature_block(c, y, x, 0, j)] for j in range(4)], axis=1)
-    for p in range(t0_ref.shape[0]):
-        piece = jnp.concatenate([t[p] for t in (t0_ref, t1_ref, t2_ref, t3_ref)], axis=1)
+    for p in range(2):
+        piece = joined(p, *piece_refs)
         out_ref[p] = lax.dot_general(weight, piece, (((1,), (1,)), ((), ())), preferred_element_type=F32)
 
 
-def project_kernel(k, t0_ref, t1_ref, t2_ref, t3_ref, w_ref, gates_ref, out_ref):
+def project_kernel(k, *refs):
+    *piece_refs, w_ref, gates_ref, out_ref = refs
     c, y, x = where_am_i()
-    rows = t0_ref.shape[1]
-    for p in range(t0_ref.shape[0]):
-        piece = jnp.concatenate([t[p] for t in (t0_ref, t1_ref, t2_ref, t3_ref)], axis=1)
+    rows = piece_refs[0].shape[1]
+    for p in range(2):
+        piece = joined(p, *piece_refs)
         total = jnp.dot(piece, w_ref[...], preferred_element_type=F32)
         out_ref[p, 0:rows, :] = total.astype(BF16)
         store_gates(out_ref, p, rows, gates_ref[p, pl.ds(scatter_head(c, y, x, k) * 8, 8), :])
@@ -170,8 +177,10 @@
 
 def small_tile(norms, totals, tops):
     norm_high = norms.astype(BF16).astype(F32)
-    parts = split_three(jnp.concatenate([totals, tops], axis=0))
-    return jnp.concatenate([norm_high, norms - norm_high, *parts], axis=0).astype(BF16)
+    high, middle, low = split_three(jnp.concatenate([totals, tops], axis=0))
+    lane = lax.broadcasted_iota(jnp.int32, high.shape, 1)
+    parts = jnp.where(lane < 32, high, jnp.where(lane < 64, middle, low))
+    return jnp.concatenate([norm_high, norms - norm_high, parts], axis=0).astype(BF16)
 
 
 def state_kernel(bias_ref, shift_ref, a_ref, b_ref, c_ref, d_ref, out_ref):
@@ -185,13 +194,17 @@
     for g in range(8):
         for i in range(4):
             out_ref[g, 16 * i : 16 * i + 16, :] = memories[i][16 * g : 16 * g + 16, :].astype(BF16)
-        out_ref[g, 64:96, :] = tile
+        out_ref[g, 64:80, :] = tile
 
 
 def merged(in_ref, count):
-    tiles = [in_ref[g, 64:96, :].astype(F32) for g in range(count)]
+    tiles = [in_ref[g, 64:80, :].astype(F32) for g in range(count)]
     norms = [t[0:4] + t[4:8] for t in tiles]
-    scalars = [t[8:16] + t[16:24] + t[24:32] for t in tiles]
+    scalars = []
+    for t in tiles:
+        parts = t[8:16]
+        whole = parts[:, 0:1] + parts[:, 32:33] + parts[:, 64:65]
+        scalars.append(jnp.broadcast_to(whole, (8, 128)))
     totals = [s[0:4] for s in scalars]
     tops = [s[4:8] for s in scalars]
     row = lax.broadcasted_iota(jnp.int32, (4, 128), 0)
@@ -227,7 +240,7 @@
     for g in range(4):
         for i in range(4):
             out_ref[g, 16 * i : 16 * i + 16, :] = blocks[i].astype(BF16)
-        out_ref[g, 64:96, :] = tile
+        out_ref[g, 64:80, :] = tile
 
 
 def last_merge_kernel(in_ref, out_ref, norm_ref, max_ref):
@@ -237,8 +250,9 @@
     for g in range(8):
         for i in range(4):
             out_ref[g, 16 * i : 16 * i + 16, :] = blocks[i].astype(BF16)
-    norm_ref[...] = norm
-    max_ref[...] = top
+    for i in range(4):
+        norm_ref[i // 2, i % 2, :, :] = norm[i : i + 1]
+        max_ref[i // 2, i % 2 : i % 2 + 1, :] = top[i : i + 1, 0:1]
 
 
 def read_kernel(in_ref, norm_ref, query_ref, matrix_ref, read_ref):
@@ -252,7 +266,7 @@
         for j in range(2):
             i = 2 * p + j
             numerator = jnp.dot(query, matrix_ref[p, j, 0], preferred_element_type=F32)
-            inner = jnp.sum(wide * norm_ref[i : i + 1, :], axis=1, keepdims=True)
+            inner = jnp.sum(wide * norm_ref[p, j, :, :], axis=1, keepdims=True)
             total = total + numerator / jnp.maximum(jnp.abs(inner), 1.0)
         read_ref[p] = total.astype(BF16)
 
@@ -260,7 +274,9 @@
 def program(tokens, w_key, w_value, w_gate, forget_bias, log_shift, new_query):
     prompts, length, width = tokens.shape
     depth = 4 * width
-    pieces = [tokens] + [gather_from(tokens, k) for k in (1, 2, 3)]
+    near = {k: gather_from(tokens, k) for k in (1, 3)}
+    far = [gather_from(near[k][p : p + 1], k) for p, k in enumerate((1, 3))]
+    pieces = [tokens, near[1], *far, near[3]]
     weights = call(pack_weights_kernel, (shape(depth, 2 * HEAD),) * 4)(w_key, w_value)
     weights = [weights[0]] + [scatter_to(weights[k], k) for k in (1, 2, 3)]
     weights = [weights[0], weights[3], weights[2], weights[1]]
@@ -278,15 +294,15 @@
         partial.append(scatter_to(part, k) if k else part)
     smem = pl.BlockSpec(memory_space=pltpu.SMEM)
     vmem = pl.BlockSpec(memory_space=pltpu.VMEM)
-    packed = call(state_kernel, shape(8, 96, HEAD), in_specs=[smem] + [vmem] * 5)(forget_bias, log_shift, *partial)
-    grouped = call(group_merge_kernel, shape(4, 96, HEAD))(exchange(packed, GROUP))
+    packed = call(state_kernel, shape(8, 80, HEAD), in_specs=[smem] + [vmem] * 5)(forget_bias, log_shift, *partial)
+    grouped = call(group_merge_kernel, shape(4, 80, HEAD))(exchange(packed, GROUP))
     slices, norm, top = call(
-        last_merge_kernel, (shape(8, 64, HEAD), shape(4, HEAD, dtype=F32), shape(4, HEAD, dtype=F32))
+        last_merge_kernel, (shape(8, 64, HEAD), shape(2, 2, 1, HEAD, dtype=F32), shape(2, 2, 1, dtype=F32))
     )(exchange(grouped, "za"))
     matrix, read = call(read_kernel, (shape(2, 2, 1, HEAD, HEAD), shape(*new_query.shape)))(
         exchange(slices, GROUP), norm, new_query
     )
-    return matrix, norm.reshape(2, 2, 1, HEAD), top[:, 0].reshape(2, 2, 1), read
+    return matrix, norm, top, read
 
 
 def solution(mesh):

time: 126 us -> 128 us (1.016)
  starting transfers between devices: 35.7 us -> 37.3 us
    ppermute x9 -> x10, starting transfers between devices: 28.7 us -> 31.2 us  [shifted(): return lax.ppermute(array, ('c', 'y', 'x'), pairs)]
    unnamed x17 -> x18, local copies, waits for them, and re-layouts: 2.72 us -> 3.38 us
    ppermute x9 -> x10, waiting for transfers between devices: 28.8 us -> 28.4 us  [shifted(): return lax.ppermute(array, ('c', 'y', 'x'), pairs)]
  transfers between devices with their start and end apart: 10 -> 11, of which waited for: 7 -> 6; matrix products, arithmetic and copies ran while one was open for 2% -> 2% of each run, Pallas kernels for 4% -> 4%
where the time goes in v1:
time: 128 us; the launch traced here: 127 us
  blocking collectives  42 us (33%)
  starting transfers between devices  37.3 us (29%)
  waiting for transfers between devices  33.6 us (26%)
  Pallas kernels  9.17 us (7%)
  local copies, waits for them, and re-layouts  4.35 us (3%)
    all_to_all x2, blocking collectives, exchange(): return lax.all_to_all(array, axes, 0, 0, tiled=True)  42 us
    ppermute x10, starting transfers between devices, shifted(): return lax.ppermute(array, ('c', 'y', 'x'), pairs)  31.2 us
    ppermute x10, waiting for transfers between devices, shifted(): return lax.ppermute(array, ('c', 'y', 'x'), pairs)  28.4 us
    all_to_all x1, starting transfers between devices, exchange(): return lax.all_to_all(array, axes, 0, 0, tiled=True)  6.07 us
    all_to_all x1, waiting for transfers between devices, exchange(): return lax.all_to_all(array, axes, 0, 0, tiled=True)  5.13 us
    pallas_call x4, Pallas kernels, program(): part = project(*pieces, weights[k], gates)  3.88 us
    unnamed x18, local copies, waits for them, and re-layouts  3.38 us
  transfers between devices with their start and end apart: 11, of which 6 were waited for; matrix products, arithmetic and copies ran while one was open for 2% of the time, Pallas kernels for 4%

profile of v1, /device:TPU:1, one launch (start us, length us, event | category | flops | bytes accessed | tf_op | source)
XLA Modules:
  0.0 127.4 jit_solution(8880089603945183503)
XLA Ops:
  0.6 5.5 %collective-permute-start.2 = (bf16[2,768,256]{2,1,0:T(8,128)(2,1)}, bf16[2,768,256]{2,1,0:T(8,128)(2,1)S(1)}, u32[]{:S(2)}, u32[]{:S(2)}) collective-permute-start(bf16[2,768,256]{2,1,0:T(8,128)(2,1)} %refs_0_.9), channel_id=1, source_target_pairs={{0,3},{1,0},{2,1},{3,2},{4,7},{5,4},{6,5},{7,6},{8,11},{9,8},{10,9... | collective-permute-start | bytes 2359304 | tf_op jit(solution)/shard_map/ppermute | solution.py:27
  6.1 1.9 %collective-permute-start = (bf16[2,768,256]{2,1,0:T(8,128)(2,1)}, bf16[2,768,256]{2,1,0:T(8,128)(2,1)S(1)}, u32[]{:S(2)}, u32[]{:S(2)}) collective-permute-start(bf16[2,768,256]{2,1,0:T(8,128)(2,1)} %refs_0_.9), channel_id=1, source_target_pairs={{0,1},{1,2},{2,3},{3,0},{4,5},{5,6},{6,7},{7,4},{8,9},{9,10},{10,1... | collective-permute-start | bytes 2359304 | tf_op jit(solution)/shard_map/ppermute | solution.py:27
  8.0 1.2 copy-done.1
  9.3 1.2 copy-done.2
  10.9 3.1 %collective-permute-start.8 = (bf16[1024,256]{1,0:T(8,128)(2,1)S(1)}, bf16[1024,256]{1,0:T(8,128)(2,1)S(1)}, u32[]{:S(2)}, u32[]{:S(2)}) collective-permute-start(bf16[1024,256]{1,0:T(8,128)(2,1)S(1)} %get-tuple-element.16), channel_id=1, source_target_pairs={{0,4},{1,5},{2,6},{3,7},{4,8},{5,9},{6,10},{7,11},{8,12},{9,13},{1... | collective-permute-start | bytes 1572872 | tf_op jit(solution)/shard_map/ppermute | solution.py:27
  14.0 3.4 %collective-permute-start.4 = (bf16[1024,256]{1,0:T(8,128)(2,1)S(1)}, bf16[1024,256]{1,0:T(8,128)(2,1)S(1)}, u32[]{:S(2)}, u32[]{:S(2)}) collective-permute-start(bf16[1024,256]{1,0:T(8,128)(2,1)S(1)} %get-tuple-element.14), channel_id=1, source_target_pairs={{0,12},{1,13},{2,14},{3,15},{4,0},{5,1},{6,2},{7,3},{8,4},{9,5},{1... | collective-permute-start | bytes 1572872 | tf_op jit(solution)/shard_map/ppermute | solution.py:27
  17.4 3.4 %collective-permute-start.6 = (bf16[1024,256]{1,0:T(8,128)(2,1)S(1)}, bf16[1024,256]{1,0:T(8,128)(2,1)S(1)}, u32[]{:S(2)}, u32[]{:S(2)}) collective-permute-start(bf16[1024,256]{1,0:T(8,128)(2,1)S(1)} %get-tuple-element.15), channel_id=1, source_target_pairs={{0,8},{1,9},{2,10},{3,11},{4,12},{5,13},{6,14},{7,15},{8,0},{9,1},... | collective-permute-start | bytes 1572872 | tf_op jit(solution)/shard_map/ppermute | solution.py:27
  20.9 4.7 %collective-permute-start.3 = (bf16[1,768,256]{2,1,0:T(8,128)(2,1)S(1)}, bf16[1,768,256]{2,1,0:T(8,128)(2,1)S(1)}, u32[]{:S(2)}, u32[]{:S(2)}) collective-permute-start(bf16[1,768,256]{2,1,0:T(8,128)(2,1)S(1)} %slice.9), channel_id=1, source_target_pairs={{0,3},{1,0},{2,1},{3,2},{4,7},{5,4},{6,5},{7,6},{8,11},{9,8},{10,9... | collective-permute-start | bytes 1179656 | tf_op jit(solution)/shard_map/ppermute | solution.py:27
  25.6 1.9 %collective-permute-start.1 = (bf16[1,768,256]{2,1,0:T(8,128)(2,1)S(1)}, bf16[1,768,256]{2,1,0:T(8,128)(2,1)S(1)}, u32[]{:S(2)}, u32[]{:S(2)}) collective-permute-start(bf16[1,768,256]{2,1,0:T(8,128)(2,1)S(1)} %slice.8), channel_id=1, source_target_pairs={{0,1},{1,2},{2,3},{3,0},{4,5},{5,6},{6,7},{7,4},{8,9},{9,10},{10,1... | collective-permute-start | bytes 1179656 | tf_op jit(solution)/shard_map/ppermute | solution.py:27
  28.9 10.5 %collective-permute-done.3.refs_3_ = bf16[1,768,256]{2,1,0:T(8,128)(2,1)S(1)} collective-permute-done((bf16[1,768,256]{2,1,0:T(8,128)(2,1)S(1)}, bf16[1,768,256]{2,1,0:T(8,128)(2,1)S(1)}, u32[]{:S(2)}, u32[]{:S(2)}) %collective-permute-start.3) | collective-permute-done | bytes 393248 | tf_op jit(solution)/shard_map/ppermute | solution.py:27
  40.1 1.1 shard_map.103.refs_6_
  42.2 2.8 %collective-permute-start.9 = (bf16[2,800,256]{2,1,0:T(8,128)(2,1)S(1)}, bf16[2,800,256]{2,1,0:T(8,128)(2,1)S(1)}, u32[]{:S(2)}, u32[]{:S(2)}) collective-permute-start(bf16[2,800,256]{2,1,0:T(8,128)(2,1)S(1)} %shard_map.107), channel_id=1, source_target_pairs={{0,12},{1,13},{2,14},{3,15},{4,0},{5,1},{6,2},{7,3},{8,4},{9,5},{1... | collective-permute-start | bytes 2457608 | tf_op jit(solution)/shard_map/ppermute | solution.py:27
  46.0 2.5 %collective-permute-start.7 = (bf16[2,800,256]{2,1,0:T(8,128)(2,1)S(1)}, bf16[2,800,256]{2,1,0:T(8,128)(2,1)S(1)}, u32[]{:S(2)}, u32[]{:S(2)}) collective-permute-start(bf16[2,800,256]{2,1,0:T(8,128)(2,1)S(1)} %shard_map.106), channel_id=1, source_target_pairs={{0,8},{1,9},{2,10},{3,11},{4,12},{5,13},{6,14},{7,15},{8,0},{9,1},... | collective-permute-start | bytes 2457608 | tf_op jit(solution)/shard_map/ppermute | solution.py:27
  48.6 1.0 shard_map.105
  49.5 1.9 %collective-permute-start.5 = (bf16[2,800,256]{2,1,0:T(8,128)(2,1)S(1)}, bf16[2,800,256]{2,1,0:T(8,128)(2,1)S(1)}, u32[]{:S(2)}, u32[]{:S(2)}) collective-permute-start(bf16[2,800,256]{2,1,0:T(8,128)(2,1)S(1)} %shard_map.105), channel_id=1, source_target_pairs={{0,4},{1,5},{2,6},{3,7},{4,8},{5,9},{6,10},{7,11},{8,12},{9,13},{1... | collective-permute-start | bytes 2457608 | tf_op jit(solution)/shard_map/ppermute | solution.py:27
  51.5 1.0 shard_map.104.a_ref
  52.5 3.1 %collective-permute-done.9.d_ref = bf16[2,800,256]{2,1,0:T(8,128)(2,1)S(1)} collective-permute-done((bf16[2,800,256]{2,1,0:T(8,128)(2,1)S(1)}, bf16[2,800,256]{2,1,0:T(8,128)(2,1)S(1)}, u32[]{:S(2)}, u32[]{:S(2)}) %collective-permute-start.9) | collective-permute-done | bytes 819232 | tf_op jit(solution)/shard_map/ppermute | solution.py:27
  55.6 5.4 %collective-permute-done.7.c_ref = bf16[2,800,256]{2,1,0:T(8,128)(2,1)S(1)} collective-permute-done((bf16[2,800,256]{2,1,0:T(8,128)(2,1)S(1)}, bf16[2,800,256]{2,1,0:T(8,128)(2,1)S(1)}, u32[]{:S(2)}, u32[]{:S(2)}) %collective-permute-start.7) | collective-permute-done | bytes 819232 | tf_op jit(solution)/shard_map/ppermute | solution.py:27
  61.0 8.7 %collective-permute-done.5.b_ref = bf16[2,800,256]{2,1,0:T(8,128)(2,1)S(1)} collective-permute-done((bf16[2,800,256]{2,1,0:T(8,128)(2,1)S(1)}, bf16[2,800,256]{2,1,0:T(8,128)(2,1)S(1)}, u32[]{:S(2)}, u32[]{:S(2)}) %collective-permute-start.5) | collective-permute-done | bytes 819232 | tf_op jit(solution)/shard_map/ppermute | solution.py:27
  69.7 1.9 %shard_map.108 = bf16[8,80,128]{2,1,0:T(8,128)(2,1)S(1)} custom-call(f32[2,16]{1,0:T(2,128)S(1)} %copy-done.6, f32[2,4,1,768]{3,2,1,0:T(1,128)S(1)} %copy-done.4, bf16[2,800,256]{2,1,0:T(8,128)(2,1)S(1)} %shard_map.104.a_ref, bf16[2,800,256]{2,1,0:T(8,128)(2,1)S(1)} %collective-permute-done.5.b_ref, bf16[2,800,256]{2,1,0:T(8,128)(2,1)S(1)} %collective-permute-done.7.c_ref, ...), custom_call_target="tpu_custom_call" | custom-call | flops 1000000 | bytes 1000000 | tf_op jit(solution)/shard_map/pallas_call | solution.py:297
  71.6 17.9 %all_to_all.15.in_ref = bf16[8,80,128]{2,1,0:T(8,128)(2,1)S(1)} all-to-all(bf16[8,80,128]{2,1,0:T(8,128)(2,1)S(1)} %shard_map.108), channel_id=1, replica_groups=mesh['za'=4,'zb'=4,'c'=2,'y'=4,'x'=4] {'zb','c'}, dimensions={0} | all-to-all | bytes 327680 | tf_op jit(solution)/shard_map/all_to_all | solution.py:51
  89.8 24.1 %all_to_all.16.in_ref = bf16[4,80,128]{2,1,0:T(8,128)(2,1)S(1)} all-to-all(bf16[4,80,128]{2,1,0:T(8,128)(2,1)S(1)} %shard_map.109), channel_id=1, replica_groups=mesh['za'=4,'zb'=4,'c'=2,'y'=4,'x'=4] {'za'}, dimensions={0} | all-to-all | bytes 163840 | tf_op jit(solution)/shard_map/all_to_all | solution.py:51
  114.7 6.1 %all-to-all-start.2 = ((bf16[8,64,128]{2,1,0:T(8,128)(2,1)}), bf16[8,64,128]{2,1,0:T(8,128)(2,1)S(1)}, u32[]{:S(2)}, u32[]{:S(2)}) async-start(bf16[8,64,128]{2,1,0:T(8,128)(2,1)} %get-tuple-element.17), calls=%async_computation.2 | async-start | bytes 262144 | tf_op jit(solution)/shard_map/all_to_all | solution.py:51
  121.4 5.1 %all-to-all-done.2.in_ref = bf16[8,64,128]{2,1,0:T(8,128)(2,1)S(1)} async-done(((bf16[8,64,128]{2,1,0:T(8,128)(2,1)}), bf16[8,64,128]{2,1,0:T(8,128)(2,1)S(1)}, u32[]{:S(2)}, u32[]{:S(2)}) %all-to-all-start.2) | async-done | bytes 131104 | tf_op jit(solution)/shard_map/all_to_all | solution.py:51
  (33 shorter events, 6.9 us)
Async XLA Ops:
  0.6 20.2 %collective-permute-start.2 = (bf16[2,768,256]{2,1,0:T(8,128)(2,1)}, bf16[2,768,256]{2,1,0:T(8,128)(2,1)S(1)}, u32[]{:S(2)}, u32[]{:S(2)}) collective-permute-start(bf16[2,768,256]{2,1,0:T(8,128)(2,1)} %refs_0_.9), channel_id=1, source_target_pairs={{0,3},{1,0},{2,1},{3,2},{4,7},{5,4},{6,5},{7,6},{8,11},{9,8},{10,9... | collective-permute-start | bytes 2359304 | tf_op jit(solution)/shard_map/ppermute | solution.py:27
  6.1 19.5 %collective-permute-start = (bf16[2,768,256]{2,1,0:T(8,128)(2,1)}, bf16[2,768,256]{2,1,0:T(8,128)(2,1)S(1)}, u32[]{:S(2)}, u32[]{:S(2)}) collective-permute-start(bf16[2,768,256]{2,1,0:T(8,128)(2,1)} %refs_0_.9), channel_id=1, source_target_pairs={{0,1},{1,2},{2,3},{3,0},{4,5},{5,6},{6,7},{7,4},{8,9},{9,10},{10,1... | collective-permute-start | bytes 2359304 | tf_op jit(solution)/shard_map/ppermute | solution.py:27
  8.0 1.2 copy-start.1
  9.3 1.2 copy-start.2
  10.9 30.4 %collective-permute-start.8 = (bf16[1024,256]{1,0:T(8,128)(2,1)S(1)}, bf16[1024,256]{1,0:T(8,128)(2,1)S(1)}, u32[]{:S(2)}, u32[]{:S(2)}) collective-permute-start(bf16[1024,256]{1,0:T(8,128)(2,1)S(1)} %get-tuple-element.16), channel_id=1, source_target_pairs={{0,4},{1,5},{2,6},{3,7},{4,8},{5,9},{6,10},{7,11},{8,12},{9,13},{1... | collective-permute-start | bytes 1572872 | tf_op jit(solution)/shard_map/ppermute | solution.py:27
  14.0 34.6 %collective-permute-start.4 = (bf16[1024,256]{1,0:T(8,128)(2,1)S(1)}, bf16[1024,256]{1,0:T(8,128)(2,1)S(1)}, u32[]{:S(2)}, u32[]{:S(2)}) collective-permute-start(bf16[1024,256]{1,0:T(8,128)(2,1)S(1)} %get-tuple-element.14), channel_id=1, source_target_pairs={{0,12},{1,13},{2,14},{3,15},{4,0},{5,1},{6,2},{7,3},{8,4},{9,5},{1... | collective-permute-start | bytes 1572872 | tf_op jit(solution)/shard_map/ppermute | solution.py:27
  17.4 27.7 %collective-permute-start.6 = (bf16[1024,256]{1,0:T(8,128)(2,1)S(1)}, bf16[1024,256]{1,0:T(8,128)(2,1)S(1)}, u32[]{:S(2)}, u32[]{:S(2)}) collective-permute-start(bf16[1024,256]{1,0:T(8,128)(2,1)S(1)} %get-tuple-element.15), channel_id=1, source_target_pairs={{0,8},{1,9},{2,10},{3,11},{4,12},{5,13},{6,14},{7,15},{8,0},{9,1},... | collective-permute-start | bytes 1572872 | tf_op jit(solution)/shard_map/ppermute | solution.py:27
  20.9 6.7 %copy-start.7 = (bf16[4096,4,16]{0,2,1:T(8,128)(2,1)S(1)}, bf16[4096,4,16]{0,2,1:T(8,128)(2,1)}, u32[]{:S(2)}) copy-start(bf16[4096,4,16]{0,2,1:T(8,128)(2,1)} %param.10) | copy-start | bytes 1572868
  20.9 18.5 %collective-permute-start.3 = (bf16[1,768,256]{2,1,0:T(8,128)(2,1)S(1)}, bf16[1,768,256]{2,1,0:T(8,128)(2,1)S(1)}, u32[]{:S(2)}, u32[]{:S(2)}) collective-permute-start(bf16[1,768,256]{2,1,0:T(8,128)(2,1)S(1)} %slice.9), channel_id=1, source_target_pairs={{0,3},{1,0},{2,1},{3,2},{4,7},{5,4},{6,5},{7,6},{8,11},{9,8},{10,9... | collective-permute-start | bytes 1179656 | tf_op jit(solution)/shard_map/ppermute | solution.py:27
  25.6 14.4 %collective-permute-start.1 = (bf16[1,768,256]{2,1,0:T(8,128)(2,1)S(1)}, bf16[1,768,256]{2,1,0:T(8,128)(2,1)S(1)}, u32[]{:S(2)}, u32[]{:S(2)}) collective-permute-start(bf16[1,768,256]{2,1,0:T(8,128)(2,1)S(1)} %slice.8), channel_id=1, source_target_pairs={{0,1},{1,2},{2,3},{3,0},{4,5},{5,6},{6,7},{7,4},{8,9},{9,10},{10,1... | collective-permute-start | bytes 1179656 | tf_op jit(solution)/shard_map/ppermute | solution.py:27
  28.5 11.6 %copy-start = (bf16[2,768,256]{2,1,0:T(8,128)(2,1)S(1)}, bf16[2,768,256]{2,1,0:T(8,128)(2,1)}, u32[]{:S(2)}) copy-start(bf16[2,768,256]{2,1,0:T(8,128)(2,1)} %refs_0_.9) | copy-start | bytes 2359300
  42.2 13.4 %collective-permute-start.9 = (bf16[2,800,256]{2,1,0:T(8,128)(2,1)S(1)}, bf16[2,800,256]{2,1,0:T(8,128)(2,1)S(1)}, u32[]{:S(2)}, u32[]{:S(2)}) collective-permute-start(bf16[2,800,256]{2,1,0:T(8,128)(2,1)S(1)} %shard_map.107), channel_id=1, source_target_pairs={{0,12},{1,13},{2,14},{3,15},{4,0},{5,1},{6,2},{7,3},{8,4},{9,5},{1... | collective-permute-start | bytes 2457608 | tf_op jit(solution)/shard_map/ppermute | solution.py:27
  46.0 14.9 %collective-permute-start.7 = (bf16[2,800,256]{2,1,0:T(8,128)(2,1)S(1)}, bf16[2,800,256]{2,1,0:T(8,128)(2,1)S(1)}, u32[]{:S(2)}, u32[]{:S(2)}) collective-permute-start(bf16[2,800,256]{2,1,0:T(8,128)(2,1)S(1)} %shard_map.106), channel_id=1, source_target_pairs={{0,8},{1,9},{2,10},{3,11},{4,12},{5,13},{6,14},{7,15},{8,0},{9,1},... | collective-permute-start | bytes 2457608 | tf_op jit(solution)/shard_map/ppermute | solution.py:27
  49.5 20.2 %collective-permute-start.5 = (bf16[2,800,256]{2,1,0:T(8,128)(2,1)S(1)}, bf16[2,800,256]{2,1,0:T(8,128)(2,1)S(1)}, u32[]{:S(2)}, u32[]{:S(2)}) collective-permute-start(bf16[2,800,256]{2,1,0:T(8,128)(2,1)S(1)} %shard_map.105), channel_id=1, source_target_pairs={{0,4},{1,5},{2,6},{3,7},{4,8},{5,9},{6,10},{7,11},{8,12},{9,13},{1... | collective-permute-start | bytes 2457608 | tf_op jit(solution)/shard_map/ppermute | solution.py:27
  51.5 18.2 %copy-start.4 = (f32[2,4,1,768]{3,2,1,0:T(1,128)S(1)}, f32[2,4,1,768]{3,2,1,0:T(1,128)}, u32[]{:S(2)}) copy-start(f32[2,4,1,768]{3,2,1,0:T(1,128)} %shift_ref.1) | copy-start | bytes 73732
  51.5 18.2 %copy-start.6 = (f32[2,16]{1,0:T(2,128)S(1)}, f32[2,16]{1,0:T(2,128)}, u32[]{:S(2)}) copy-start(f32[2,16]{1,0:T(2,128)} %bias_ref.1) | copy-start | bytes 388
  114.7 11.9 %copy-start.3 = (bf16[2,128,128]{2,1,0:T(8,128)(2,1)S(1)}, bf16[2,128,128]{2,1,0:T(8,128)(2,1)}, u32[]{:S(2)}) copy-start(bf16[2,128,128]{2,1,0:T(8,128)(2,1)} %query_ref.1) | copy-start | bytes 196612
  114.7 11.9 %all-to-all-start.2 = ((bf16[8,64,128]{2,1,0:T(8,128)(2,1)}), bf16[8,64,128]{2,1,0:T(8,128)(2,1)S(1)}, u32[]{:S(2)}, u32[]{:S(2)}) async-start(bf16[8,64,128]{2,1,0:T(8,128)(2,1)} %get-tuple-element.17), calls=%async_computation.2 | async-start | bytes 262144 | tf_op jit(solution)/shard_map/all_to_all | solution.py:51
  120.7 5.8 %copy-start.5 = (f32[2,2,1,128]{3,2,1,0:T(1,128)S(1)}, f32[2,2,1,128]{3,2,1,0:T(1,128)}, u32[]{:S(2)}) copy-start(f32[2,2,1,128]{3,2,1,0:T(1,128)} %get-tuple-element.27.norm_ref) | copy-start | bytes 6148

commit v2 on v1

--- a/solution.py
+++ b/solution.py
@@ -65,14 +65,29 @@
     return jax.ShapeDtypeStruct(dims, dtype)
 
 
+def first_of_pair():
+    return lax.axis_index("zb") % 2 == 0
+
+
 def pack_weights_kernel(wk_ref, wv_ref, *out_refs):
     c, y, x = where_am_i()
     part = out_refs[0].shape[0] // 4
     for k, out in enumerate(out_refs):
         for j in range(4):
             rows = pl.ds(feature_block(c, y, x, k, j) * part, part)
-            out[j * part : (j + 1) * part, 0:128] = wk_ref[rows, :]
-            out[j * part : (j + 1) * part, 128:256] = wv_ref[rows, :]
+            here = slice(j * part, (j + 1) * part)
+            if k == 2:
+
+                @pl.when(first_of_pair())
+                def _(out=out, here=here, rows=rows):
+                    out[here, :] = wk_ref[rows, :]
+
+                @pl.when(jnp.logical_not(first_of_pair()))
+                def _(out=out, here=here, rows=rows):
+                    out[here, :] = wv_ref[rows, :]
+            else:
+                out[here, 0:128] = wk_ref[rows, :]
+                out[here, 128:256] = wv_ref[rows, :]
 
 
 def pair_rows(values):
@@ -109,12 +124,18 @@
 
 
 def project_kernel(k, *refs):
-    *piece_refs, w_ref, gates_ref, out_ref = refs
+    *in_refs, gates_ref, out_ref = refs
+    piece_refs, w_refs = in_refs[:5], in_refs[5:]
     c, y, x = where_am_i()
     rows = piece_refs[0].shape[1]
+    weight = jnp.concatenate([w[...] for w in w_refs], axis=1)
     for p in range(2):
         piece = joined(p, *piece_refs)
-        total = jnp.dot(piece, w_ref[...], preferred_element_type=F32)
+        total = jnp.dot(piece, weight, preferred_element_type=F32)
+        if len(w_refs) == 2:
+            own, other = total[:, 0:128], total[:, 128:256]
+            first = first_of_pair()
+            total = jnp.concatenate([jnp.where(first, own, other), jnp.where(first, other, own)], axis=1)
         out_ref[p, 0:rows, :] = total.astype(BF16)
         store_gates(out_ref, p, rows, gates_ref[p, pl.ds(scatter_head(c, y, x, k) * 8, 8), :])
 
@@ -252,7 +273,7 @@
             out_ref[g, 16 * i : 16 * i + 16, :] = blocks[i].astype(BF16)
     for i in range(4):
         norm_ref[i // 2, i % 2, :, :] = norm[i : i + 1]
-        max_ref[i // 2, i % 2 : i % 2 + 1, :] = top[i : i + 1, 0:1]
+        max_ref[i // 2, :, i % 2 : i % 2 + 1] = top[i : i + 1, 0:1]
 
 
 def read_kernel(in_ref, norm_ref, query_ref, matrix_ref, read_ref):
@@ -277,11 +298,14 @@
     near = {k: gather_from(tokens, k) for k in (1, 3)}
     far = [gather_from(near[k][p : p + 1], k) for p, k in enumerate((1, 3))]
     pieces = [tokens, near[1], *far, near[3]]
-    weights = call(pack_weights_kernel, (shape(depth, 2 * HEAD),) * 4)(w_key, w_value)
+    packed_shapes = tuple(shape(depth, HEAD if k == 2 else 2 * HEAD) for k in range(4))
+    weights = call(pack_weights_kernel, packed_shapes)(w_key, w_value)
     weights = [weights[0]] + [scatter_to(weights[k], k) for k in (1, 2, 3)]
-    weights = [weights[0], weights[3], weights[2], weights[1]]
     gate = w_gate.transpose(2, 1, 0)
     gate = jnp.concatenate([gate, gate], axis=1).reshape(128, 16, width).transpose(1, 0, 2)
+    weights[2], gate = lax.optimization_barrier((weights[2], gate))
+    swapped = lax.ppermute(weights[2], "zb", [(i, i ^ 1) for i in range(4)])
+    weights = [(weights[0],), (weights[3],), (weights[2], swapped), (weights[1],)]
     gates = call(gates_kernel, shape(prompts, 128, length, dtype=F32))(*pieces, gate)
     partial = []
     for k in range(4):
@@ -290,19 +314,19 @@
             shape(prompts, length + 32, 2 * HEAD),
             flops=2 * prompts * length * depth * 256,
         )
-        part = project(*pieces, weights[k], gates)
+        part = project(*pieces, *weights[k], gates)
         partial.append(scatter_to(part, k) if k else part)
     smem = pl.BlockSpec(memory_space=pltpu.SMEM)
     vmem = pl.BlockSpec(memory_space=pltpu.VMEM)
     packed = call(state_kernel, shape(8, 80, HEAD), in_specs=[smem] + [vmem] * 5)(forget_bias, log_shift, *partial)
     grouped = call(group_merge_kernel, shape(4, 80, HEAD))(exchange(packed, GROUP))
     slices, norm, top = call(
-        last_merge_kernel, (shape(8, 64, HEAD), shape(2, 2, 1, HEAD, dtype=F32), shape(2, 2, 1, dtype=F32))
+        last_merge_kernel, (shape(8, 64, HEAD), shape(2, 2, 1, HEAD, dtype=F32), shape(2, 1, 2, dtype=F32))
     )(exchange(grouped, "za"))
     matrix, read = call(read_kernel, (shape(2, 2, 1, HEAD, HEAD), shape(*new_query.shape)))(
         exchange(slices, GROUP), norm, new_query
     )
-    return matrix, norm, top, read
+    return matrix, norm, top.transpose(0, 2, 1), read
 
 
 def solution(mesh):

time: 128 us -> 122 us (0.953)
  waiting for transfers between devices: 33.6 us -> 20.9 us
  blocking collectives: 42 us -> 51 us
  starting transfers between devices: 37.3 us -> 35.8 us
    all_to_all x2 -> x3, blocking collectives: 42 us -> 51 us  [exchange(): return lax.all_to_all(array, axes, 0, 0, tiled=True)]
    ppermute x10, waiting for transfers between devices: 28.4 us -> 20.9 us  [shifted(): return lax.ppermute(array, ('c', 'y', 'x'), pairs)]
    all_to_all x1 -> x0, starting transfers between devices: 6.07 us -> none  [exchange(): return lax.all_to_all(array, axes, 0, 0, tiled=True)]
    all_to_all x1 -> x0, waiting for transfers between devices: 5.13 us -> none  [exchange(): return lax.all_to_all(array, axes, 0, 0, tiled=True)]
    ppermute x0 -> x1, starting transfers between devices: none -> 3.55 us  [program(): swapped = lax.ppermute(weights[2], 'zb', [(i, i ^ 1) for i in range(4)])]
    unnamed x18 -> x17, local copies, waits for them, and re-layouts: 3.38 us -> 2.72 us
  transfers between devices with their start and end apart: 11 -> 11, of which waited for: 6 -> 4; matrix products, arithmetic and copies ran while one was open for 2% -> 1% of each run, Pallas kernels for 4% -> 4%
where the time goes in v2:
time: 122 us; the launch traced here: 121 us
  blocking collectives  51 us (42%)
  starting transfers between devices  35.8 us (29%)
  waiting for transfers between devices  20.9 us (17%)
  Pallas kernels  9.1 us (7%)
  local copies, waits for them, and re-layouts  3.7 us (3%)
    all_to_all x3, blocking collectives, exchange(): return lax.all_to_all(array, axes, 0, 0, tiled=True)  51 us
    ppermute x10, starting transfers between devices, shifted(): return lax.ppermute(array, ('c', 'y', 'x'), pairs)  32.3 us
    ppermute x10, waiting for transfers between devices, shifted(): return lax.ppermute(array, ('c', 'y', 'x'), pairs)  20.9 us
    pallas_call x4, Pallas kernels, program(): part = project(*pieces, *weights[k], gates)  3.88 us
    ppermute x1, starting transfers between devices, program(): swapped = lax.ppermute(weights[2], 'zb', [(i, i ^ 1) for i in range(4)])  3.55 us
    unnamed x17, local copies, waits for them, and re-layouts  2.72 us
  transfers between devices with their start and end apart: 11, of which 4 were waited for; matrix products, arithmetic and copies ran while one was open for 1% of the time, Pallas kernels for 4%

profile of v2, /device:TPU:1, one launch (start us, length us, event | category | flops | bytes accessed | tf_op | source)
XLA Modules:
  0.0 121.5 jit_solution(3509791659386069658)
XLA Ops:
  0.6 5.5 %collective-permute-start.2 = (bf16[2,768,256]{2,1,0:T(8,128)(2,1)}, bf16[2,768,256]{2,1,0:T(8,128)(2,1)S(1)}, u32[]{:S(2)}, u32[]{:S(2)}) collective-permute-start(bf16[2,768,256]{2,1,0:T(8,128)(2,1)} %refs_0_.9), channel_id=1, source_target_pairs={{0,3},{1,0},{2,1},{3,2},{4,7},{5,4},{6,5},{7,6},{8,11},{9,8},{10,9... | collective-permute-start | bytes 2359304 | tf_op jit(solution)/shard_map/ppermute | solution.py:27
  6.1 1.9 %collective-permute-start = (bf16[2,768,256]{2,1,0:T(8,128)(2,1)}, bf16[2,768,256]{2,1,0:T(8,128)(2,1)S(1)}, u32[]{:S(2)}, u32[]{:S(2)}) collective-permute-start(bf16[2,768,256]{2,1,0:T(8,128)(2,1)} %refs_0_.9), channel_id=1, source_target_pairs={{0,1},{1,2},{2,3},{3,0},{4,5},{5,6},{6,7},{7,4},{8,9},{9,10},{10,1... | collective-permute-start | bytes 2359304 | tf_op jit(solution)/shard_map/ppermute | solution.py:27
  8.0 1.2 %copy-done.1 = bf16[4096,128]{1,0:T(8,128)(2,1)S(1)} copy-done((bf16[4096,128]{1,0:T(8,128)(2,1)S(1)}, bf16[4096,128]{1,0:T(8,128)(2,1)}, u32[]{:S(2)}) %copy-start.1) | copy-done | bytes 1048600
  9.3 1.2 %copy-done.2 = bf16[4096,128]{1,0:T(8,128)(2,1)S(1)} copy-done((bf16[4096,128]{1,0:T(8,128)(2,1)S(1)}, bf16[4096,128]{1,0:T(8,128)(2,1)}, u32[]{:S(2)}) %copy-start.2) | copy-done | bytes 1048600
  10.8 4.7 %collective-permute-start.4 = (bf16[1024,128]{1,0:T(8,128)(2,1)S(1)}, bf16[1024,128]{1,0:T(8,128)(2,1)S(1)}, u32[]{:S(2)}, u32[]{:S(2)}) collective-permute-start(bf16[1024,128]{1,0:T(8,128)(2,1)S(1)} %get-tuple-element.16), channel_id=1, source_target_pairs={{0,8},{1,9},{2,10},{3,11},{4,12},{5,13},{6,14},{7,15},{8,0},{9,1},... | collective-permute-start | bytes 786440 | tf_op jit(solution)/shard_map/ppermute | solution.py:27
  15.5 2.8 %collective-permute-start.5 = (bf16[1024,256]{1,0:T(8,128)(2,1)S(1)}, bf16[1024,256]{1,0:T(8,128)(2,1)S(1)}, u32[]{:S(2)}, u32[]{:S(2)}) collective-permute-start(bf16[1024,256]{1,0:T(8,128)(2,1)S(1)} %get-tuple-element.18), channel_id=1, source_target_pairs={{0,12},{1,13},{2,14},{3,15},{4,0},{5,1},{6,2},{7,3},{8,4},{9,5},{1... | collective-permute-start | bytes 1572872 | tf_op jit(solution)/shard_map/ppermute | solution.py:27
  18.3 2.5 %collective-permute-start.9 = (bf16[1024,256]{1,0:T(8,128)(2,1)S(1)}, bf16[1024,256]{1,0:T(8,128)(2,1)S(1)}, u32[]{:S(2)}, u32[]{:S(2)}) collective-permute-start(bf16[1024,256]{1,0:T(8,128)(2,1)S(1)} %get-tuple-element.20), channel_id=1, source_target_pairs={{0,4},{1,5},{2,6},{3,7},{4,8},{5,9},{6,10},{7,11},{8,12},{9,13},{1... | collective-permute-start | bytes 1572872 | tf_op jit(solution)/shard_map/ppermute | solution.py:27
  20.9 4.7 %collective-permute-start.3 = (bf16[1,768,256]{2,1,0:T(8,128)(2,1)S(1)}, bf16[1,768,256]{2,1,0:T(8,128)(2,1)S(1)}, u32[]{:S(2)}, u32[]{:S(2)}) collective-permute-start(bf16[1,768,256]{2,1,0:T(8,128)(2,1)S(1)} %slice.9), channel_id=1, source_target_pairs={{0,3},{1,0},{2,1},{3,2},{4,7},{5,4},{6,5},{7,6},{8,11},{9,8},{10,9... | collective-permute-start | bytes 1179656 | tf_op jit(solution)/shard_map/ppermute | solution.py:27
  25.6 1.9 %collective-permute-start.1 = (bf16[1,768,256]{2,1,0:T(8,128)(2,1)S(1)}, bf16[1,768,256]{2,1,0:T(8,128)(2,1)S(1)}, u32[]{:S(2)}, u32[]{:S(2)}) collective-permute-start(bf16[1,768,256]{2,1,0:T(8,128)(2,1)S(1)} %slice.8), channel_id=1, source_target_pairs={{0,1},{1,2},{2,3},{3,0},{4,5},{5,6},{6,7},{7,4},{8,9},{9,10},{10,1... | collective-permute-start | bytes 1179656 | tf_op jit(solution)/shard_map/ppermute | solution.py:27
  28.9 3.5 %collective-permute-start.7 = (bf16[1024,128]{1,0:T(8,128)(2,1)S(1)}, bf16[1024,128]{1,0:T(8,128)(2,1)S(1)}, u32[]{:S(2)}, u32[]{:S(2)}) collective-permute-start(bf16[1024,128]{1,0:T(8,128)(2,1)S(1)} %collective-permute-done.4.refs_5_), channel_id=1, source_target_pairs={{0,32},{32,0},{64,96},{96,64},{1,33},{33,1},{65,97},{97,65},{2,34}... | collective-permute-start | bytes 786440 | tf_op jit(solution)/shard_map/ppermute | solution.py:307
  33.0 4.0 %collective-permute-done.1.refs_2_ = bf16[1,768,256]{2,1,0:T(8,128)(2,1)S(1)} collective-permute-done((bf16[1,768,256]{2,1,0:T(8,128)(2,1)S(1)}, bf16[1,768,256]{2,1,0:T(8,128)(2,1)S(1)}, u32[]{:S(2)}, u32[]{:S(2)}) %collective-permute-start.1) | collective-permute-done | bytes 393248 | tf_op jit(solution)/shard_map/ppermute | solution.py:27
  36.9 1.1 shard_map.103.refs_6_.refs_7_
  38.1 1.0 shard_map.107
  39.1 3.3 %collective-permute-start.10 = (bf16[2,800,256]{2,1,0:T(8,128)(2,1)S(1)}, bf16[2,800,256]{2,1,0:T(8,128)(2,1)S(1)}, u32[]{:S(2)}, u32[]{:S(2)}) collective-permute-start(bf16[2,800,256]{2,1,0:T(8,128)(2,1)S(1)} %shard_map.107), channel_id=1, source_target_pairs={{0,12},{1,13},{2,14},{3,15},{4,0},{5,1},{6,2},{7,3},{8,4},{9,5},{1... | collective-permute-start | bytes 2457608 | tf_op jit(solution)/shard_map/ppermute | solution.py:27
  42.4 1.0 shard_map.105
  43.4 1.9 %collective-permute-start.6 = (bf16[2,800,256]{2,1,0:T(8,128)(2,1)S(1)}, bf16[2,800,256]{2,1,0:T(8,128)(2,1)S(1)}, u32[]{:S(2)}, u32[]{:S(2)}) collective-permute-start(bf16[2,800,256]{2,1,0:T(8,128)(2,1)S(1)} %shard_map.105), channel_id=1, source_target_pairs={{0,4},{1,5},{2,6},{3,7},{4,8},{5,9},{6,10},{7,11},{8,12},{9,13},{1... | collective-permute-start | bytes 2457608 | tf_op jit(solution)/shard_map/ppermute | solution.py:27
  45.4 1.0 shard_map.106
  46.3 3.1 %collective-permute-start.8 = (bf16[2,800,256]{2,1,0:T(8,128)(2,1)S(1)}, bf16[2,800,256]{2,1,0:T(8,128)(2,1)S(1)}, u32[]{:S(2)}, u32[]{:S(2)}) collective-permute-start(bf16[2,800,256]{2,1,0:T(8,128)(2,1)S(1)} %shard_map.106), channel_id=1, source_target_pairs={{0,8},{1,9},{2,10},{3,11},{4,12},{5,13},{6,14},{7,15},{8,0},{9,1},... | collective-permute-start | bytes 2457608 | tf_op jit(solution)/shard_map/ppermute | solution.py:27
  50.4 2.0 %collective-permute-done.10.d_ref = bf16[2,800,256]{2,1,0:T(8,128)(2,1)S(1)} collective-permute-done((bf16[2,800,256]{2,1,0:T(8,128)(2,1)S(1)}, bf16[2,800,256]{2,1,0:T(8,128)(2,1)S(1)}, u32[]{:S(2)}, u32[]{:S(2)}) %collective-permute-start.10) | collective-permute-done | bytes 819232 | tf_op jit(solution)/shard_map/ppermute | solution.py:27
  52.5 14.3 %collective-permute-done.6.b_ref = bf16[2,800,256]{2,1,0:T(8,128)(2,1)S(1)} collective-permute-done((bf16[2,800,256]{2,1,0:T(8,128)(2,1)S(1)}, bf16[2,800,256]{2,1,0:T(8,128)(2,1)S(1)}, u32[]{:S(2)}, u32[]{:S(2)}) %collective-permute-start.6) | collective-permute-done | bytes 819232 | tf_op jit(solution)/shard_map/ppermute | solution.py:27
  66.8 1.9 %shard_map.108 = bf16[8,80,128]{2,1,0:T(8,128)(2,1)S(1)} custom-call(f32[2,16]{1,0:T(2,128)S(1)} %copy-done.6, f32[2,4,1,768]{3,2,1,0:T(1,128)S(1)} %copy-done.4, bf16[2,800,256]{2,1,0:T(8,128)(2,1)S(1)} %shard_map.104.a_ref, bf16[2,800,256]{2,1,0:T(8,128)(2,1)S(1)} %collective-permute-done.6.b_ref, bf16[2,800,256]{2,1,0:T(8,128)(2,1)S(1)} %collective-permute-done.8.c_ref, ...), custom_call_target="tpu_custom_call" | custom-call | flops 1000000 | bytes 1000000 | tf_op jit(solution)/shard_map/pallas_call | solution.py:321
  68.7 15.3 %all_to_all.15.in_ref = bf16[8,80,128]{2,1,0:T(8,128)(2,1)S(1)} all-to-all(bf16[8,80,128]{2,1,0:T(8,128)(2,1)S(1)} %shard_map.108), channel_id=1, replica_groups=mesh['za'=4,'zb'=4,'c'=2,'y'=4,'x'=4] {'zb','c'}, dimensions={0} | all-to-all | bytes 327680 | tf_op jit(solution)/shard_map/all_to_all | solution.py:51
  84.2 24.1 %all_to_all.16.in_ref = bf16[4,80,128]{2,1,0:T(8,128)(2,1)S(1)} all-to-all(bf16[4,80,128]{2,1,0:T(8,128)(2,1)S(1)} %shard_map.109), channel_id=1, replica_groups=mesh['za'=4,'zb'=4,'c'=2,'y'=4,'x'=4] {'za'}, dimensions={0} | all-to-all | bytes 163840 | tf_op jit(solution)/shard_map/all_to_all | solution.py:51
  109.0 11.6 %all_to_all.17.in_ref = bf16[8,64,128]{2,1,0:T(8,128)(2,1)S(1)} all-to-all(bf16[8,64,128]{2,1,0:T(8,128)(2,1)S(1)} %get-tuple-element.21), channel_id=1, replica_groups=mesh['za'=4,'zb'=4,'c'=2,'y'=4,'x'=4] {'zb','c'}, dimensions={0} | all-to-all | bytes 262144 | tf_op jit(solution)/shard_map/all_to_all | solution.py:51
  (33 shorter events, 5.0 us)
Async XLA Ops:
  0.6 20.2 %collective-permute-start.2 = (bf16[2,768,256]{2,1,0:T(8,128)(2,1)}, bf16[2,768,256]{2,1,0:T(8,128)(2,1)S(1)}, u32[]{:S(2)}, u32[]{:S(2)}) collective-permute-start(bf16[2,768,256]{2,1,0:T(8,128)(2,1)} %refs_0_.9), channel_id=1, source_target_pairs={{0,3},{1,0},{2,1},{3,2},{4,7},{5,4},{6,5},{7,6},{8,11},{9,8},{10,9... | collective-permute-start | bytes 2359304 | tf_op jit(solution)/shard_map/ppermute | solution.py:27
  6.1 19.5 %collective-permute-start = (bf16[2,768,256]{2,1,0:T(8,128)(2,1)}, bf16[2,768,256]{2,1,0:T(8,128)(2,1)S(1)}, u32[]{:S(2)}, u32[]{:S(2)}) collective-permute-start(bf16[2,768,256]{2,1,0:T(8,128)(2,1)} %refs_0_.9), channel_id=1, source_target_pairs={{0,1},{1,2},{2,3},{3,0},{4,5},{5,6},{6,7},{7,4},{8,9},{9,10},{10,1... | collective-permute-start | bytes 2359304 | tf_op jit(solution)/shard_map/ppermute | solution.py:27
  8.0 1.2 %copy-start.1 = (bf16[4096,128]{1,0:T(8,128)(2,1)S(1)}, bf16[4096,128]{1,0:T(8,128)(2,1)}, u32[]{:S(2)}) copy-start(bf16[4096,128]{1,0:T(8,128)(2,1)} %wk_ref.1) | copy-start | bytes 3145732
  9.3 1.2 %copy-start.2 = (bf16[4096,128]{1,0:T(8,128)(2,1)S(1)}, bf16[4096,128]{1,0:T(8,128)(2,1)}, u32[]{:S(2)}) copy-start(bf16[4096,128]{1,0:T(8,128)(2,1)} %wv_ref.1) | copy-start | bytes 3145732
  10.8 18.0 %collective-permute-start.4 = (bf16[1024,128]{1,0:T(8,128)(2,1)S(1)}, bf16[1024,128]{1,0:T(8,128)(2,1)S(1)}, u32[]{:S(2)}, u32[]{:S(2)}) collective-permute-start(bf16[1024,128]{1,0:T(8,128)(2,1)S(1)} %get-tuple-element.16), channel_id=1, source_target_pairs={{0,8},{1,9},{2,10},{3,11},{4,12},{5,13},{6,14},{7,15},{8,0},{9,1},... | collective-permute-start | bytes 786440 | tf_op jit(solution)/shard_map/ppermute | solution.py:27
  15.5 26.9 %collective-permute-start.5 = (bf16[1024,256]{1,0:T(8,128)(2,1)S(1)}, bf16[1024,256]{1,0:T(8,128)(2,1)S(1)}, u32[]{:S(2)}, u32[]{:S(2)}) collective-permute-start(bf16[1024,256]{1,0:T(8,128)(2,1)S(1)} %get-tuple-element.18), channel_id=1, source_target_pairs={{0,12},{1,13},{2,14},{3,15},{4,0},{5,1},{6,2},{7,3},{8,4},{9,5},{1... | collective-permute-start | bytes 1572872 | tf_op jit(solution)/shard_map/ppermute | solution.py:27
  18.3 19.8 %collective-permute-start.9 = (bf16[1024,256]{1,0:T(8,128)(2,1)S(1)}, bf16[1024,256]{1,0:T(8,128)(2,1)S(1)}, u32[]{:S(2)}, u32[]{:S(2)}) collective-permute-start(bf16[1024,256]{1,0:T(8,128)(2,1)S(1)} %get-tuple-element.20), channel_id=1, source_target_pairs={{0,4},{1,5},{2,6},{3,7},{4,8},{5,9},{6,10},{7,11},{8,12},{9,13},{1... | collective-permute-start | bytes 1572872 | tf_op jit(solution)/shard_map/ppermute | solution.py:27
  20.8 6.7 %copy-start.7 = (bf16[4096,4,16]{0,2,1:T(8,128)(2,1)S(1)}, bf16[4096,4,16]{0,2,1:T(8,128)(2,1)}, u32[]{:S(2)}) copy-start(bf16[4096,4,16]{0,2,1:T(8,128)(2,1)} %param.10) | copy-start | bytes 1572868
  20.9 12.1 %collective-permute-start.3 = (bf16[1,768,256]{2,1,0:T(8,128)(2,1)S(1)}, bf16[1,768,256]{2,1,0:T(8,128)(2,1)S(1)}, u32[]{:S(2)}, u32[]{:S(2)}) collective-permute-start(bf16[1,768,256]{2,1,0:T(8,128)(2,1)S(1)} %slice.9), channel_id=1, source_target_pairs={{0,3},{1,0},{2,1},{3,2},{4,7},{5,4},{6,5},{7,6},{8,11},{9,8},{10,9... | collective-permute-start | bytes 1179656 | tf_op jit(solution)/shard_map/ppermute | solution.py:27
  25.6 11.3 %collective-permute-start.1 = (bf16[1,768,256]{2,1,0:T(8,128)(2,1)S(1)}, bf16[1,768,256]{2,1,0:T(8,128)(2,1)S(1)}, u32[]{:S(2)}, u32[]{:S(2)}) collective-permute-start(bf16[1,768,256]{2,1,0:T(8,128)(2,1)S(1)} %slice.8), channel_id=1, source_target_pairs={{0,1},{1,2},{2,3},{3,0},{4,5},{5,6},{6,7},{7,4},{8,9},{9,10},{10,1... | collective-permute-start | bytes 1179656 | tf_op jit(solution)/shard_map/ppermute | solution.py:27
  28.5 8.4 %copy-start = (bf16[2,768,256]{2,1,0:T(8,128)(2,1)S(1)}, bf16[2,768,256]{2,1,0:T(8,128)(2,1)}, u32[]{:S(2)}) copy-start(bf16[2,768,256]{2,1,0:T(8,128)(2,1)} %refs_0_.9) | copy-start | bytes 2359300
  28.9 16.5 %collective-permute-start.7 = (bf16[1024,128]{1,0:T(8,128)(2,1)S(1)}, bf16[1024,128]{1,0:T(8,128)(2,1)S(1)}, u32[]{:S(2)}, u32[]{:S(2)}) collective-permute-start(bf16[1024,128]{1,0:T(8,128)(2,1)S(1)} %collective-permute-done.4.refs_5_), channel_id=1, source_target_pairs={{0,32},{32,0},{64,96},{96,64},{1,33},{33,1},{65,97},{97,65},{2,34}... | collective-permute-start | bytes 786440 | tf_op jit(solution)/shard_map/ppermute | solution.py:307
  39.1 13.4 %collective-permute-start.10 = (bf16[2,800,256]{2,1,0:T(8,128)(2,1)S(1)}, bf16[2,800,256]{2,1,0:T(8,128)(2,1)S(1)}, u32[]{:S(2)}, u32[]{:S(2)}) collective-permute-start(bf16[2,800,256]{2,1,0:T(8,128)(2,1)S(1)} %shard_map.107), channel_id=1, source_target_pairs={{0,12},{1,13},{2,14},{3,15},{4,0},{5,1},{6,2},{7,3},{8,4},{9,5},{1... | collective-permute-start | bytes 2457608 | tf_op jit(solution)/shard_map/ppermute | solution.py:27
  43.4 23.4 %collective-permute-start.6 = (bf16[2,800,256]{2,1,0:T(8,128)(2,1)S(1)}, bf16[2,800,256]{2,1,0:T(8,128)(2,1)S(1)}, u32[]{:S(2)}, u32[]{:S(2)}) collective-permute-start(bf16[2,800,256]{2,1,0:T(8,128)(2,1)S(1)} %shard_map.105), channel_id=1, source_target_pairs={{0,4},{1,5},{2,6},{3,7},{4,8},{5,9},{6,10},{7,11},{8,12},{9,13},{1... | collective-permute-start | bytes 2457608 | tf_op jit(solution)/shard_map/ppermute | solution.py:27
  46.3 20.4 %collective-permute-start.8 = (bf16[2,800,256]{2,1,0:T(8,128)(2,1)S(1)}, bf16[2,800,256]{2,1,0:T(8,128)(2,1)S(1)}, u32[]{:S(2)}, u32[]{:S(2)}) collective-permute-start(bf16[2,800,256]{2,1,0:T(8,128)(2,1)S(1)} %shard_map.106), channel_id=1, source_target_pairs={{0,8},{1,9},{2,10},{3,11},{4,12},{5,13},{6,14},{7,15},{8,0},{9,1},... | collective-permute-start | bytes 2457608 | tf_op jit(solution)/shard_map/ppermute | solution.py:27
  49.4 17.4 %copy-start.4 = (f32[2,4,1,768]{3,2,1,0:T(1,128)S(1)}, f32[2,4,1,768]{3,2,1,0:T(1,128)}, u32[]{:S(2)}) copy-start(f32[2,4,1,768]{3,2,1,0:T(1,128)} %shift_ref.1) | copy-start | bytes 73732
  49.4 17.3 %copy-start.6 = (f32[2,16]{1,0:T(2,128)S(1)}, f32[2,16]{1,0:T(2,128)}, u32[]{:S(2)}) copy-start(f32[2,16]{1,0:T(2,128)} %bias_ref.1) | copy-start | bytes 388
  109.0 11.6 %copy-start.3 = (bf16[2,128,128]{2,1,0:T(8,128)(2,1)S(1)}, bf16[2,128,128]{2,1,0:T(8,128)(2,1)}, u32[]{:S(2)}) copy-start(bf16[2,128,128]{2,1,0:T(8,128)(2,1)} %query_ref.1) | copy-start | bytes 196612
  109.0 11.6 %copy-start.5 = (f32[2,2,1,128]{3,2,1,0:T(1,128)S(1)}, f32[2,2,1,128]{3,2,1,0:T(1,128)}, u32[]{:S(2)}) copy-start(f32[2,2,1,128]{3,2,1,0:T(1,128)} %get-tuple-element.31.norm_ref) | copy-start | bytes 6148
